TPU v7x, 128 devices: a whole 4x4x4 slice. The times are simulated.
128 devices in a mesh: sp: 64 (over z, y, x), tp: 2 (over core).
Axes of the slice: x: 4, y: 4, z: 4, core: 2. Of those that a mesh axis runs over, the one named last changes fastest.
Arguments:
- residual: bfloat16 [8192, 2048], P(('sp', 'tp')), may hold values from -6 to 6
- conv_input: bfloat16 [8192, 1024], P('sp', 'tp'), may hold values from -6 to 6
- input_gate: bfloat16 [8192, 1024], P('sp', 'tp'), may hold values from -6 to 6
- output_gate: bfloat16 [8192, 1024], P('sp', 'tp'), may hold values from -6 to 6
- conv_taps: bfloat16 [3, 1024], P(None, 'tp'), may hold values from -3.5 to 3.5
- out_proj: bfloat16 [1024, 2048], P('tp'), may hold values from -0.1875 to 0.1875
- norm_gain: float32 [2048], replicated, may hold values from 0.1 to 1.9
- routes: int32 [8192, 2], P(('sp', 'tp')), may hold values from 0 to 63, all different within a row; in each aligned block of 64 rows (0 to 63, 64 to 127, ...) at most 4 rows name the same one
- route_weight: float32 [8192, 2], P(('sp', 'tp')), may hold values from 0.1 to 1
- gate_proj: bfloat16 [64, 2048, 3584], P('sp', None, 'tp'), may hold values from -0.125 to 0.125
- up_proj: bfloat16 [64, 2048, 3584], P('sp', None, 'tp'), may hold values from -0.125 to 0.125
- down_proj: bfloat16 [64, 3584, 2048], P('sp', 'tp'), may hold values from -0.09375 to 0.09375
Outputs:
- layer_out: bfloat16 [8192, 2048], P(('sp', 'tp'))
Inputs may be any that keep to these rules, and one draw needn't show every extreme that they name: `routes`: A token's 2 experts differ. Among the 64 tokens of one device, in the aligned blocks of the tokens' order, no expert is named more than 4 times, a bound that some block reaches in some device.
All inputs are finite; a program needn't handle non-finite values.
Results may differ from a plain program's by a relative error of at most 0.0054.
Values may be sent and summed in bfloat16 or wider, within the bound.
A program may use at most 128 MiB of HBM per device.

v0:
```python
import jax
import jax.numpy as jnp
from jax import lax
from jax.sharding import PartitionSpec as P


def from_behind(value, axis, by):
    peers = lax.axis_size(axis)
    pairs = [(i, i + by) for i in range(peers) if 0 <= i + by < peers]
    return lax.ppermute(value, axis, pairs)


def in_blocks(value, dim, peers):
    before, after = (value.shape[:dim], value.shape[dim + 1 :])
    return jnp.moveaxis(value.reshape(*before, peers, -1, *after), dim, 0)


def summed_on_arrival(value, axis, dim):
    parts = in_blocks(value, dim, lax.axis_size(axis))
    arrived = lax.all_to_all(parts, axis, split_axis=0, concat_axis=0, tiled=True)
    return arrived.sum(axis=0)


def from_everyone(value, axis):
    peers = lax.axis_size(axis)
    return lax.all_to_all(
        jnp.broadcast_to(value[None], (peers, *value.shape)), axis, 0, 0, tiled=True
    )


def joined_along(parts, dim):
    parts = jnp.moveaxis(parts, 0, dim)
    dims = parts.shape
    return parts.reshape(*dims[:dim], dims[dim] * dims[dim + 1], *dims[dim + 2 :])


def collect(value, axis, dim):
    parts = from_everyone(value, axis)
    return joined_along(parts, dim)


def sum_at_owner(value, axis, dim):
    parts = in_blocks(value, dim, lax.axis_size(axis))
    arrived = lax.all_to_all(parts, axis, split_axis=0, concat_axis=0, tiled=True)
    return arrived.astype(jnp.float32).sum(axis=0)


def expert_rows(flat_rows, gate_proj, up_proj, down_proj):
    gate_val = jnp.dot(flat_rows, gate_proj[0], preferred_element_type=jnp.float32)
    up_val = jnp.dot(flat_rows, up_proj[0], preferred_element_type=jnp.float32)
    active = (jax.nn.silu(gate_val) * up_val).astype(jnp.bfloat16)
    return jnp.dot(active, down_proj[0], preferred_element_type=jnp.float32).astype(jnp.bfloat16)


def per_device(
    residual,
    conv_input,
    input_gate,
    output_gate,
    conv_taps,
    out_proj,
    norm_gain,
    routes,
    route_weight,
    gate_proj,
    up_proj,
    down_proj,
):
    tap_count = conv_taps.shape[0]
    length = conv_input.shape[0]
    rim_rows = jnp.stack(
        [conv_input[length - tap_count + 1 :], input_gate[length - tap_count + 1 :]]
    )
    before = from_behind(rim_rows, "sp", 1)
    ext_input = jnp.concatenate([before[0], conv_input], axis=0)
    ext_gate = jnp.concatenate([before[1], input_gate], axis=0)
    mixed = ext_gate.astype(jnp.float32) * ext_input.astype(jnp.float32)
    convolved = jnp.zeros((length, mixed.shape[1]), jnp.float32)
    for tap_index in range(tap_count):
        convolved = (
            convolved
            + conv_taps[tap_index].astype(jnp.float32)[None, :]
            * mixed[tap_index : tap_index + length]
        )
    gated_rows = (output_gate.astype(jnp.float32) * convolved).astype(jnp.bfloat16)
    picked = gated_rows
    projected = summed_on_arrival(
        jnp.dot(picked, out_proj, preferred_element_type=jnp.float32), "tp", 0
    )
    stream = residual.astype(jnp.float32) + projected
    inverse_rms = lax.rsqrt(jnp.mean(stream * stream, axis=-1, keepdims=True) + 1e-06)
    normed = (stream * inverse_rms * norm_gain[None, :]).astype(jnp.bfloat16)
    experts = lax.axis_size("sp")
    groups = lax.axis_size("tp")
    tok_rows = normed.shape[0]
    width = normed.shape[1]
    top_count = routes.shape[1]
    capacity = 2 * tok_rows * top_count // experts
    flat_routes = routes.reshape(-1)
    onehot = (flat_routes[:, None] == jnp.arange(experts, dtype=jnp.int32)[None, :]).astype(
        jnp.int32
    )
    slot_ids = jnp.sum(onehot * (jnp.cumsum(onehot, axis=0) - 1), axis=1)
    target = flat_routes * capacity + slot_ids
    spread = jnp.broadcast_to(normed[:, None, :], (tok_rows, top_count, width)).reshape(
        tok_rows * top_count, width
    )
    outgoing = jnp.zeros((experts * capacity, width), jnp.bfloat16).at[target].set(spread)
    gathered = collect(
        lax.all_to_all(
            outgoing.reshape(experts, 1, capacity, width),
            "sp",
            split_axis=0,
            concat_axis=0,
            tiled=True,
        ),
        "tp",
        1,
    )
    slot_count = gathered.shape[2]
    ordered = jnp.transpose(gathered, (1, 0, 2, 3)).reshape(groups * experts * slot_count, width)
    picked = ordered
    kept = sum_at_owner(
        expert_rows(picked, gate_proj, up_proj, down_proj).astype(jnp.float32).astype(jnp.bfloat16),
        "tp",
        0,
    )
    kept = kept.astype(jnp.bfloat16).reshape(experts, slot_count, width)
    returned = lax.all_to_all(kept, "sp", split_axis=0, concat_axis=0, tiled=True)
    summed = returned.astype(jnp.float32).reshape(experts * capacity, width)
    values = summed[target].reshape(tok_rows, top_count, width)
    routed = jnp.sum(route_weight[:, :, None] * values, axis=1)
    return (stream + routed).astype(jnp.bfloat16)


def solution(mesh):
    return jax.shard_map(
        per_device,
        mesh=mesh,
        in_specs=(
            P(("sp", "tp"), None),
            P("sp", "tp"),
            P("sp", "tp"),
            P("sp", "tp"),
            P(None, "tp"),
            P("tp", None),
            P(),
            P(("sp", "tp"), None),
            P(("sp", "tp"), None),
            P("sp", None, "tp"),
            P("sp", None, "tp"),
            P("sp", "tp", None),
        ),
        out_specs=P(("sp", "tp"), None),
        check_vma=False,
    )
```

profile of v0, /device:TPU:0, one launch (start us, length us, event | category | flops | bytes accessed | tf_op | source)
XLA Modules:
  0.0 143.6 jit_solution(5326536517277204506)
XLA Ops:
  0.0 0.9 slice_bitcast_fusion.2
  0.9 3.5 %collective-permute-start = (bf16[2,2,512]{2,1,0:T(2,128)(2,1)S(1)}, bf16[2,2,512]{2,1,0:T(2,128)(2,1)S(1)}, u32[]{:S(2)}, u32[]{:S(2)}) collective-permute-start(bf16[2,2,512]{2,1,0:T(2,128)(2,1)S(1)} %pad_maximum_fusion), channel_id=1, source_target_pairs={{0,2},{2,4},{4,6},{6,8},{8,10},{10,12},{12,14},{14,16},{16,18},{18... | collective-permute-start | bytes 12296 | tf_op jit(solution)/shard_map/ppermute | solution.py:10
  4.4 0.8 copy.21
  5.2 0.7 broadcast_multiply_fusion
  5.9 0.8 slice_convert_fusion.2
  6.9 0.2 reduce_window_sum.11
  7.1 0.2 select_reduce_fusion
  7.5 1.0 convert_multiply_fusion
  8.6 1.4 fusion.19
  10.0 5.4 %all_to_all.25 = f32[2,64,2048]{2,1,0:T(8,128)} all-to-all(f32[2,64,2048]{2,1,0:T(8,128)S(1)} %bitcast.45), channel_id=1, replica_groups=mesh['sp'=64,'tp'=2] {'tp'}, dimensions={0} | all-to-all | bytes 2097152 | tf_op jit(solution)/shard_map/all_to_all | solution.py:20
  15.4 1.3 reduce_sum.50
  16.8 0.2 multiply_reduce_fusion.1
  17.1 0.3 broadcast_in_dim.9
  17.4 1.0 reshape.101
  18.4 3.0 %scatter_custom_fusion = bf16[256,2048]{1,0:T(8,128)(2,1)} fusion(s32[128]{0:T(128)S(1)} %fusion.25, bf16[128,2048]{1,0:T(8,128)(2,1)} %reshape.101, bf16[]{:T(256)} %constant.7.clone.1), kind=kCustom, calls=%fused_computation.14 | custom fusion | bytes 1049088 | tf_op jit(solution)/shard_map/scatter | solution.py:108
  21.4 2.3 %reshape.76 = bf16[64,1,4,2048]{3,2,1,0:T(4,128)(2,1)} reshape(bf16[256,2048]{1,0:T(8,128)(2,1)} %scatter_custom_fusion) | data formatting | bytes 2097152 | tf_op jit(solution)/shard_map/reshape | solution.py:111
  23.6 30.3 %all_to_all.26 = bf16[64,1,4,2048]{3,2,1,0:T(4,128)(2,1)S(1)} all-to-all(bf16[64,1,4,2048]{3,2,1,0:T(4,128)(2,1)} %reshape.76), channel_id=1, replica_groups=mesh['sp'=64,'tp'=2] {'sp'}, dimensions={0} | all-to-all | bytes 2097152 | tf_op jit(solution)/shard_map/all_to_all | solution.py:110
  54.0 1.1 broadcast_in_dim.11
  55.0 6.3 %all_to_all.27 = bf16[2,64,1,4,2048]{4,3,2,1,0:T(4,128)(2,1)} all-to-all(bf16[2,64,1,4,2048]{4,3,2,1,0:T(4,128)(2,1)S(1)} %broadcast_in_dim.11), channel_id=1, replica_groups=mesh['sp'=64,'tp'=2] {'tp'}, dimensions={0} | all-to-all | bytes 4194304 | tf_op jit(solution)/shard_map/all_to_all | solution.py:26
  61.3 4.0 %reshape.78 = bf16[512,2048]{1,0:T(8,128)(2,1)} reshape(bf16[2,64,4,2048]{3,2,1,0:T(4,128)(2,1)} %bitcast.43) | data formatting | bytes 4194304 | tf_op jit(solution)/shard_map/reshape | solution.py:121
  65.3 9.5 %fusion.4 = f32[512,1792]{1,0:T(8,128)} fusion(bf16[512,2048]{1,0:T(8,128)(2,1)} %reshape.78, bf16[1,2048,1792]{2,1,0:T(8,128)(2,1)} %param.21), kind=kOutput, calls=%fused_computation.6 | convolution fusion | flops 3758096384 | bytes 13107200 | tf_op jit(solution)/shard_map/dot_general | solution.py:49
  74.8 17.0 %fusion.8 = bf16[512,2048]{1,0:T(8,128)(2,1)} fusion(bf16[1,1792,2048]{2,1,0:T(8,128)(2,1)} %param.23, f32[512,1792]{1,0:T(8,128)} %fusion.4, bf16[512,2048]{1,0:T(8,128)(2,1)} %reshape.78, bf16[1,2048,1792]{2,1,0:T(8,128)(2,1)} %param.22), kind=kOutput, calls=%fused_computation.9 | convolution fusion | flops 7522746368 | bytes 22544384 | tf_op jit(solution)/shard_map/dot_general | solution.py:52
  91.7 8.6 %all_to_all.28 = bf16[2,256,2048]{2,1,0:T(8,128)(2,1)} all-to-all(bf16[2,256,2048]{2,1,0:T(8,128)(2,1)} %bitcast.46), channel_id=1, replica_groups=mesh['sp'=64,'tp'=2] {'tp'}, dimensions={0} | all-to-all | bytes 4194304 | tf_op jit(solution)/shard_map/all_to_all | solution.py:44
  100.3 3.3 %reduce_sum.54 = bf16[256,2048]{1,0:T(8,128)(2,1)} reduce(bf16[2,256,2048]{2,1,0:T(8,128)(2,1)} %all_to_all.28, bf16[]{:T(256)} %constant.7.clone.1), dimensions={0}, to_apply=%region_5.6 | reduce | flops 524288 | bytes 3145730 | tf_op jit(solution)/shard_map/reduce_sum | solution.py:45
  103.6 2.3 %reshape.80 = bf16[64,4,2048]{2,1,0:T(4,128)(2,1)} reshape(bf16[256,2048]{1,0:T(8,128)(2,1)} %reduce_sum.54) | data formatting | bytes 2097152 | tf_op jit(solution)/shard_map/reshape | solution.py:128
  105.9 5.7 %all-to-all-start.4 = ((bf16[64,4,2048]{2,1,0:T(4,128)(2,1)}), bf16[64,4,2048]{2,1,0:T(4,128)(2,1)}, u32[]{:S(2)}, u32[]{:S(2)}) async-start(bf16[64,4,2048]{2,1,0:T(4,128)(2,1)} %reshape.80), calls=%async_computation.4 | async-start | bytes 2097152 | tf_op jit(solution)/shard_map/all_to_all | solution.py:129
  111.7 19.0 %all-to-all-done.4 = bf16[64,4,2048]{2,1,0:T(4,128)(2,1)} async-done(((bf16[64,4,2048]{2,1,0:T(4,128)(2,1)}), bf16[64,4,2048]{2,1,0:T(4,128)(2,1)}, u32[]{:S(2)}, u32[]{:S(2)}) %all-to-all-start.4) | async-done | bytes 1048608 | tf_op jit(solution)/shard_map/all_to_all | solution.py:129
  130.7 2.5 %reshape.88 = f32[256,2048]{1,0:T(8,128)} reshape(bf16[64,4,2048]{2,1,0:T(4,128)(2,1)} %all-to-all-done.4) | data formatting | bytes 3145728 | tf_op jit(solution)/shard_map/reshape | solution.py:130
  133.2 4.0 %gather_fusion = f32[128,2048]{1,0:T(8,128)} fusion(f32[256,2048]{1,0:T(8,128)} %reshape.88, s32[1024]{0:T(1024)S(1)} %pad_clamp_fusion), kind=kCustom, calls=%fused_computation | custom fusion | bytes 2097664 | tf_op jit(solution)/shard_map/gather | solution.py:131
  137.2 2.8 %reshape.83 = f32[64,2,2048]{2,1,0:T(2,128)} reshape(f32[128,2048]{1,0:T(8,128)} %gather_fusion) | data formatting | bytes 2097152 | tf_op jit(solution)/shard_map/reshape | solution.py:131
  140.0 2.8 %multiply_reduce_fusion = f32[64,2048]{1,0:T(8,128)S(1)} fusion(f32[64,2,2048]{2,1,0:T(2,128)} %reshape.83, f32[64,2]{1,0:T(8,128)S(1)} %copy.19), kind=kLoop, calls=%fused_computation.10 | loop fusion | flops 393216 | bytes 1573376 | tf_op jit(solution)/shard_map/reduce_sum | solution.py:132
  142.8 0.8 add_convert_fusion
  (20 shorter events, 0.7 us)
Async XLA Ops:
  0.0 8.6 %copy-start = (bf16[512,2048]{1,0:T(8,128)(2,1)S(1)}, bf16[512,2048]{1,0:T(8,128)(2,1)}, u32[]{:S(2)}) copy-start(bf16[512,2048]{1,0:T(8,128)(2,1)} %param.17) | copy-start | bytes 6291460
  0.9 6.6 %collective-permute-start = (bf16[2,2,512]{2,1,0:T(2,128)(2,1)S(1)}, bf16[2,2,512]{2,1,0:T(2,128)(2,1)S(1)}, u32[]{:S(2)}, u32[]{:S(2)}) collective-permute-start(bf16[2,2,512]{2,1,0:T(2,128)(2,1)S(1)} %pad_maximum_fusion), channel_id=1, source_target_pairs={{0,2},{2,4},{4,6},{6,8},{8,10},{10,12},{12,14},{14,16},{16,18},{18... | collective-permute-start | bytes 12296 | tf_op jit(solution)/shard_map/ppermute | solution.py:10
  8.6 8.2 %copy-start.1 = (bf16[64,2048]{1,0:T(8,128)(2,1)S(1)}, bf16[64,2048]{1,0:T(8,128)(2,1)}, u32[]{:S(2)}) copy-start(bf16[64,2048]{1,0:T(8,128)(2,1)} %param.12) | copy-start | bytes 786436
  8.6 8.4 %copy-start.2 = (f32[2048]{0:T(1024)S(1)}, f32[2048]{0:T(1024)}, u32[]{:S(2)}) copy-start(f32[2048]{0:T(1024)} %param.18) | copy-start | bytes 24580
  100.3 11.3 %copy-start.3 = (f32[64,2]{0,1:T(2,128)S(1)}, f32[64,2]{0,1:T(2,128)}, u32[]{:S(2)}) copy-start(f32[64,2]{0,1:T(2,128)} %param.20) | copy-start | bytes 1540
  105.9 24.8 %all-to-all-start.4 = ((bf16[64,4,2048]{2,1,0:T(4,128)(2,1)}), bf16[64,4,2048]{2,1,0:T(4,128)(2,1)}, u32[]{:S(2)}, u32[]{:S(2)}) async-start(bf16[64,4,2048]{2,1,0:T(4,128)(2,1)} %reshape.80), calls=%async_computation.4 | async-start | bytes 2097152 | tf_op jit(solution)/shard_map/all_to_all | solution.py:129
where the time goes:
time: 145 us; the launch traced here: 144 us
  blocking collectives  50.6 us (35%)
  matrix products  27.9 us (19%)
  local copies, waits for them, and re-layouts  25.3 us (17%)
  waiting for transfers between devices  19 us (13%)
  other arithmetic  11.5 us (8%)
  starting transfers between devices  9.24 us (6%)
    all_to_all x1, blocking collectives, per_device(): lax.all_to_all(outgoing.reshape(experts, 1, capacity, width), 'sp', split...  30.3 us
    all_to_all x1, waiting for transfers between devices, per_device(): lax.all_to_all(kept, 'sp', split_axis=0, concat_axis=0, tiled=True)  19 us
    dot_general x1, matrix products, expert_rows(): jnp.dot(active, down_proj[0], preferred_element_type=jnp.float32)  17 us
    dot_general x1, matrix products, expert_rows(): jnp.dot(flat_rows, gate_proj[0], preferred_element_type=jnp.float32)  9.47 us
    all_to_all x1, blocking collectives, sum_at_owner(): lax.all_to_all(parts, axis, split_axis=0, concat_axis=0, tiled=True)  8.57 us
    all_to_all x1, blocking collectives, from_everyone(): lax.all_to_all(jnp.broadcast_to(value[None], (peers, *value.shape)), axis...  6.31 us
    all_to_all x1, starting transfers between devices, per_device(): lax.all_to_all(kept, 'sp', split_axis=0, concat_axis=0, tiled=True)  5.73 us
    all_to_all x1, blocking collectives, summed_on_arrival(): lax.all_to_all(parts, axis, split_axis=0, concat_axis=0, tiled=True)  5.36 us
  transfers between devices with their start and end apart: 2, of which 1 were waited for; matrix products, arithmetic and copies ran while one was open for 2% of the time, Pallas kernels for 0%

commit v1 on v0

v1 whole, which is shorter than its diff:
```python
import functools

import jax
import jax.numpy as jnp
from jax import lax
from jax.experimental import pallas as pl
from jax.experimental.pallas import tpu as pltpu
from jax.sharding import PartitionSpec as P

MESH = pl.DeviceIdType.MESH
F32, BF16, I32 = jnp.float32, jnp.bfloat16, jnp.int32
SIDE = 4
GROUPS = 4
SLABS = 16
SLOTS = 4
QUARTERS = 4
ROWS = SLABS * QUARTERS * SLOTS
EPS = 1e-06


def ring_distance(a):
    return min(a, SIDE - a)


def offsets_far_first(g):
    found = [(dz, dy, (g - dz - dy) % SIDE) for dz in range(SIDE) for dy in range(SIDE)]
    return sorted(found, key=lambda o: -sum(ring_distance(a) for a in o))


def iota(shape, dim):
    return lax.broadcasted_iota(I32, shape, dim)


def dot(a, b):
    return jnp.dot(a, b, preferred_element_type=F32)


def kernel(
    res_h, cin_h, gin_h, gout_h, taps_ref, oproj_h, gain_ref, routes_ref, weight_ref,
    wg_h, wu_h, wd_h, out_ref,
    cin_v, gin_v, gout_v, res_v, op_v, wg_v, wu_v, wd_v, halo, part, pxr, stream, n4,
    send, rown, roth, rsend, rret, x_v, h_v, yown, pps, ppr, u_v, ut_v, comb,
    in_sem, w_sem, halo_s, halo_r, px_s, px_r, dsp_s, dsp_r, fwd_s, fwd_r, pp_s, pp_r, ret_s, ret_r,
):
    sp, tp = lax.axis_index("sp"), lax.axis_index("tp")
    z, y, x = lax.div(sp, 16), lax.rem(lax.div(sp, 4), 4), lax.rem(sp, 4)
    other = 1 - tp
    rows, tok = cin_v.shape[0], res_v.shape[0]
    width, hidden = out_ref.shape[1], h_v.shape[1]
    piece = width // QUARTERS

    def remote(src, dst, s, r, **where):
        return pltpu.make_async_remote_copy(
            src_ref=src, dst_ref=dst, send_sem=s, recv_sem=r, device_id=where, device_id_type=MESH
        )

    loads = [
        pltpu.make_async_copy(a, b, in_sem.at[i])
        for i, (a, b) in enumerate(
            [(cin_h, cin_v), (gin_h, gin_v), (gout_h, gout_v), (oproj_h, op_v), (res_h, res_v)]
        )
    ]
    for load in loads:
        load.start()

    barrier = pltpu.get_barrier_semaphore()
    peers = SIDE**3

    def greet(i, carry):
        pl.semaphore_signal(
            barrier, inc=1, device_id={"sp": lax.rem(sp + i + 1, peers)}, device_id_type=MESH
        )
        return carry

    lax.fori_loop(0, peers - 1, greet, 0)
    pl.semaphore_signal(barrier, inc=1, device_id={"tp": other}, device_id_type=MESH)

    def weight_copies(i, src, dst, cuts):
        size = dst.shape[0] // cuts
        return [
            pltpu.make_async_copy(
                src.at[0, pl.ds(k * size, size)], dst.at[pl.ds(k * size, size)], w_sem.at[i]
            )
            for k in range(cuts)
        ]

    for i, (src, dst) in enumerate([(wg_h, wg_v), (wu_h, wu_v), (wd_h, wd_v)]):
        for copy in weight_copies(i, src, dst, 4):
            copy.start()

    routes = routes_ref[...].astype(F32)
    r0c, r1c = routes[:, 0:1], routes[:, 1:2]
    lanes = QUARTERS * tok
    trow, tcol = iota((tok, lanes), 0), lax.rem(iota((tok, lanes), 1), tok)
    same, before = trow == tcol, trow < tcol
    keys = []
    for rc in (r0c, r1c):
        rrow = jnp.sum(jnp.where(same, rc, 0.0), axis=0, keepdims=True)
        hits = ((r0c == rrow) | (r1c == rrow)) & before
        rank = jnp.sum(jnp.where(hits, 1.0, 0.0), axis=0, keepdims=True).astype(I32)
        e = rrow.astype(I32)
        dz = (lax.shift_right_logical(e, 4) + SIDE - z) & 3
        dy = ((lax.shift_right_logical(e, 2) & 3) + SIDE - y) & 3
        dx = ((e & 3) + SIDE - x) & 3
        keys.append((((dz + dy + dx) & 3) * SLABS + dz * SIDE + dy) * SLOTS + rank)
    first = trow == iota((tok, lanes), 1)
    key_cols = [
        jnp.sum(jnp.where(first, k.astype(F32), 0.0), axis=1, keepdims=True).astype(I32) for k in keys
    ]

    a, b = iota((ROWS, ROWS), 0), iota((ROWS, ROWS), 1)

    def plain_to_slab(r):
        q, i, s = lax.shift_right_logical(r, 6), lax.shift_right_logical(r, 2) & 15, r & 3
        return i * 16 + q * 4 + s

    u_v[...] = jnp.where(plain_to_slab(a) == b, 1.0, 0.0).astype(BF16)
    ut_v[...] = jnp.where(plain_to_slab(b) == a, 1.0, 0.0).astype(BF16)

    taps = taps_ref[...].astype(F32)
    t0, t1, t2 = taps[0:1], taps[1:2], taps[2:3]
    for load in loads[:3]:
        load.wait()
    mixed = gin_v[...].astype(F32) * cin_v[...].astype(F32)
    row = iota(mixed.shape, 0)
    m1 = jnp.where(row < 1, 0.0, pltpu.roll(mixed, 1, 0))
    m2 = jnp.where(row < 2, 0.0, pltpu.roll(mixed, 2, 0))
    gated = (gout_v[...].astype(F32) * (t0 * m2 + t1 * m1 + t2 * mixed)).astype(BF16)
    loads[3].wait()
    part[...] = dot(gated, op_v[...])

    pl.semaphore_wait(barrier, peers)
    behind = lax.rem(sp + 1, peers)
    halos = [
        remote(v.at[pl.ds(rows - 16, 16)], halo.at[i], halo_s.at[i], halo_r.at[i], sp=behind)
        for i, v in enumerate((cin_v, gin_v))
    ]
    for copy in halos:
        copy.start()
    theirs = pl.multiple_of(other * tok, tok)
    spans = [(0, 16), (16, tok - 16)]
    swaps = [
        remote(
            part.at[pl.ds(pl.multiple_of(theirs + lo, 16), n)], pxr.at[pl.ds(lo, n)],
            px_s.at[i], px_r.at[i], tp=other,
        )
        for i, (lo, n) in enumerate(spans)
    ]
    swaps[1].start()
    for copy in halos:
        copy.wait()
    hm = jnp.where(sp > 0, halo[0].astype(F32) * halo[1].astype(F32), 0.0)
    ext = jnp.concatenate([hm, gin_v[0:16].astype(F32) * cin_v[0:16].astype(F32)], axis=0)
    conv = t0 * pltpu.roll(ext, 2, 0)[16:32] + t1 * pltpu.roll(ext, 1, 0)[16:32] + t2 * ext[16:32]
    part[0:16] = dot((gout_v[0:16].astype(F32) * conv).astype(BF16), op_v[...])
    swaps[0].start()
    loads[4].wait()
    for copy in swaps:
        copy.wait()
    s = part[pl.ds(pl.multiple_of(tp * tok, tok), tok)] + pxr[...] + res_v[...].astype(F32)
    stream[...] = s
    inverse = lax.rsqrt(jnp.mean(s * s, axis=-1, keepdims=True) + EPS)
    normed = (s * inverse * gain_ref[...]).astype(BF16)
    for q in range(QUARTERS):
        n4[q * tok : (q + 1) * tok] = normed[:, q * piece : (q + 1) * piece]

    def peer(sign, dz, dy, dx):
        return (
            lax.rem(z + (sign * dz) % SIDE, SIDE) * 16
            + lax.rem(y + (sign * dy) % SIDE, SIDE) * 4
            + lax.rem(x + (sign * dx) % SIDE, SIDE)
        )

    slab_of = lax.shift_right_logical(a, 4) * SLOTS + (a & 3)
    quarter_ok = (lax.shift_right_logical(a, 2) & 3) == lax.shift_right_logical(b, 6)
    for g in range(GROUPS):
        want = slab_of + g * SLABS * SLOTS
        pick = jnp.where(((keys[0] == want) | (keys[1] == want)) & quarter_ok, 1.0, 0.0).astype(BF16)
        send[g * SLABS : (g + 1) * SLABS] = dot(pick, n4[...]).astype(BF16).reshape(SLABS, 16, piece)
        for dz, dy, dx in offsets_far_first(g):
            pos = g * SLABS + dz * SIDE + dy
            if pos:
                remote(send.at[pos], rown.at[pos], dsp_s, dsp_r.at[g], sp=peer(1, dz, dy, dx)).start()
            else:
                pltpu.make_async_copy(send.at[0], rown.at[0], dsp_r.at[0]).start()

    def group(ref, g):
        return ref.at[pl.ds(g * SLABS, SLABS)]

    def forward(g):
        return remote(group(rown, g), group(roth, g), fwd_s.at[g], fwd_r.at[g], tp=other)

    def arrived(ref, sems, g):
        return remote(group(ref, g), group(ref, g), sems.at[g], sems.at[g], tp=other)

    def halves(g):
        return remote(pps.at[g], ppr.at[g], pp_s.at[g], pp_r.at[g], tp=other)

    arrived(rown, dsp_r, 0).wait_recv()
    forward(0).start()
    for i, (src, dst) in enumerate([(wg_h, wg_v), (wu_h, wu_v), (wd_h, wd_v)]):
        pltpu.make_async_copy(src.at[0], dst, w_sem.at[i]).wait()

    by_plane = sorted(
        [(dz, dy) for dz in range(SIDE) for dy in range(SIDE)],
        key=lambda o: -sum(ring_distance(k) for k in o),
    )

    def expert(g, carry):
        forward(g).wait_recv()
        for half, ref in enumerate((rown, roth)):
            slabs = ref[pl.ds(g * SLABS, SLABS)].reshape(ROWS, piece)
            plain = dot(u_v[...], slabs).astype(BF16)
            for q in range(QUARTERS):
                x_v[half * tok : (half + 1) * tok, q * piece : (q + 1) * piece] = plain[
                    q * tok : (q + 1) * tok
                ]
        for n in range(hidden // 256):
            cols = slice(n * 256, (n + 1) * 256)
            gate, up = dot(x_v[...], wg_v[:, cols]), dot(x_v[...], wu_v[:, cols])
            h_v[:, cols] = (gate / (1.0 + jnp.exp(-gate)) * up).astype(BF16)
        for q in range(QUARTERS):
            cols = slice(q * piece, (q + 1) * piece)
            res = dot(h_v[...], wd_v[:, cols]).astype(BF16)
            yown[q * tok : (q + 1) * tok] = res[:tok]
            pps[g, q * tok : (q + 1) * tok] = res[tok:]
        halves(g).start()

        @pl.when(g < GROUPS - 1)
        def _():
            arrived(rown, dsp_r, g + 1).wait_recv()
            forward(g + 1).start()

        halves(g).wait_recv()
        total = (yown[...].astype(F32) + ppr[g].astype(F32)).astype(BF16)
        rsend[pl.ds(g * SLABS, SLABS)] = dot(ut_v[...], total).astype(BF16).reshape(SLABS, 16, piece)
        for dz, dy in by_plane:
            pos = g * SLABS + dz * SIDE + dy
            dx = lax.rem(g + 2 * SIDE - dz - dy, SIDE)
            dst = (
                lax.rem(z + SIDE - dz, SIDE) * 16
                + lax.rem(y + SIDE - dy, SIDE) * 4
                + lax.rem(x + SIDE - dx, SIDE)
            )

            def back(pos=pos, dst=dst):
                remote(rsend.at[pos], rret.at[pos], ret_s, ret_r.at[g], sp=dst).start()

            if dz or dy:
                back()
            else:
                pl.when(g > 0)(back)

                @pl.when(g == 0)
                def _():
                    pltpu.make_async_copy(rsend.at[0], rret.at[0], ret_r.at[0]).start()

        return carry

    lax.fori_loop(0, GROUPS, expert, 0)

    lane = iota((tok, ROWS), 1)
    lane_slot = lax.shift_right_logical(lane, 4) * SLOTS + (lane & 3)
    lane_quarter = lax.shift_right_logical(lane, 2) & 3
    weights = weight_ref[...]
    w0, w1 = weights[:, 0:1], weights[:, 1:2]
    comb[...] = jnp.zeros_like(comb)

    def combine(g, carry):
        want = lane_slot + g * SLABS * SLOTS
        mix = jnp.where(key_cols[0] == want, w0, 0.0) + jnp.where(key_cols[1] == want, w1, 0.0)
        high = mix.astype(BF16).astype(F32)
        low = mix - high
        pieces = [
            jnp.where(lane_quarter == q, m, 0.0).astype(BF16) for m in (high, low) for q in range(QUARTERS)
        ]
        arrived(rret, ret_r, g).wait_recv()
        slabs = rret[pl.ds(g * SLABS, SLABS)].reshape(ROWS, piece)
        comb[...] += dot(jnp.concatenate(pieces, axis=0), slabs)
        return carry

    lax.fori_loop(0, GROUPS, combine, 0)
    for q in range(QUARTERS):
        cols = slice(q * piece, (q + 1) * piece)
        routed = comb[q * tok : (q + 1) * tok] + comb[(QUARTERS + q) * tok : (QUARTERS + q + 1) * tok]
        out_ref[:, cols] = (stream[:, cols] + routed).astype(BF16)

    rest = pl.ds(1, GROUPS * SLABS - 1)
    remote(send.at[rest], rown.at[rest], dsp_s, dsp_s, tp=other).wait_send()
    remote(rsend.at[rest], rret.at[rest], ret_s, ret_s, tp=other).wait_send()
    for g in range(GROUPS):
        forward(g).wait_send()
        halves(g).wait_send()


def per_device(
    residual, conv_input, input_gate, output_gate, conv_taps, out_proj, norm_gain, routes,
    route_weight, gate_proj, up_proj, down_proj,
):
    rows, chan = conv_input.shape
    tok, width = residual.shape
    hidden = gate_proj.shape[2]
    piece = width // QUARTERS
    slabs = (GROUPS * SLABS, QUARTERS * SLOTS, piece)
    anyspace = pl.BlockSpec(memory_space=pl.ANY)
    vmem = pl.BlockSpec(memory_space=pltpu.VMEM)
    dma = pltpu.SemaphoreType.DMA
    v = pltpu.VMEM
    return pl.pallas_call(
        kernel,
        out_shape=jax.ShapeDtypeStruct((tok, width), BF16),
        in_specs=[
            anyspace, anyspace, anyspace, anyspace, vmem, anyspace, vmem, vmem, vmem,
            anyspace, anyspace, anyspace,
        ],
        out_specs=vmem,
        scratch_shapes=[
            v((rows, chan), BF16), v((rows, chan), BF16), v((rows, chan), BF16),
            v((tok, width), BF16), v((chan, width), BF16),
            v((width, hidden), BF16), v((width, hidden), BF16), v((hidden, width), BF16),
            v((2, 16, chan), BF16), v((rows, width), F32), v((tok, width), F32), v((tok, width), F32),
            v((QUARTERS * tok, piece), BF16),
            v(slabs, BF16), v(slabs, BF16), v(slabs, BF16), v(slabs, BF16), v(slabs, BF16),
            v((2 * tok, width), BF16), v((2 * tok, hidden), BF16), v((ROWS, piece), BF16),
            v((GROUPS, ROWS, piece), BF16), v((GROUPS, ROWS, piece), BF16),
            v((ROWS, ROWS), BF16), v((ROWS, ROWS), BF16), v((2 * ROWS, piece), F32),
            dma((5,)), dma((3,)), dma((2,)), dma((2,)), dma((2,)), dma((2,)),
            dma, dma((GROUPS,)), dma((GROUPS,)), dma((GROUPS,)), dma((GROUPS,)), dma((GROUPS,)),
            dma, dma((GROUPS,)),
        ],
        compiler_params=pltpu.CompilerParams(
            collective_id=0, has_side_effects=True, vmem_limit_bytes=60 * 2**20
        ),
        name="layer",
    )(
        residual, conv_input, input_gate, output_gate, conv_taps, out_proj, norm_gain.reshape(1, -1),
        routes, route_weight, gate_proj, up_proj, down_proj,
    )


def solution(mesh):
    return jax.shard_map(
        per_device,
        mesh=mesh,
        in_specs=(
            P(("sp", "tp"), None),
            P("sp", "tp"),
            P("sp", "tp"),
            P("sp", "tp"),
            P(None, "tp"),
            P("tp", None),
            P(),
            P(("sp", "tp"), None),
            P(("sp", "tp"), None),
            P("sp", None, "tp"),
            P("sp", None, "tp"),
            P("sp", "tp", None),
        ),
        out_specs=P(("sp", "tp"), None),
        check_vma=False,
    )
```

time: 145 us -> 57.1 us (0.39)
  the two profiles are of different devices: /device:TPU:0 before, /device:TPU:1 now
where the time goes in v1:
time: 57.1 us; the launch traced here: 56.9 us
  Pallas kernels  52.4 us (92%)
  local copies, waits for them, and re-layouts  4.42 us (8%)
    pallas_call x1, Pallas kernels, per_device(): pl.pallas_call(kernel, out_shape=jax.ShapeDtypeStruct((tok, width), BF16)...  52.4 us
    unnamed x3, local copies, waits for them, and re-layouts  4.42 us

profile of v1, /device:TPU:1, one launch (start us, length us, event | category | flops | bytes accessed | tf_op | source)
XLA Modules:
  0.0 56.9 jit_solution(9886403961197601690)
XLA Ops:
  0.0 1.4 %copy.13.routes_ref = s32[64,2]{1,0:T(8,128)} copy(s32[64,2]{0,1:T(2,128)} %param.19) | data formatting | bytes 1024 | tf_op args[7]
  1.4 1.4 %copy.14.weight_ref = f32[64,2]{1,0:T(8,128)} copy(f32[64,2]{0,1:T(2,128)} %param.20) | data formatting | bytes 1024 | tf_op args[8]
  2.7 52.4 %layer.1 = bf16[64,2048]{1,0:T(8,128)(2,1)} custom-call(bf16[64,2048]{1,0:T(8,128)(2,1)} %res_h.1, bf16[128,512]{1,0:T(8,128)(2,1)} %cin_h.1, bf16[128,512]{1,0:T(8,128)(2,1)} %gin_h.1, bf16[128,512]{1,0:T(8,128)(2,1)} %gout_h.1, bf16[3,512]{1,0:T(4,128)(2,1)} %taps_ref.1, bf16[512,2048]{1,0:T(8,128)(2,1)} %oproj_h.1, f32[1,2048]{1,0:T(1,128)} %bitcast.1, ...), custom_call_target="tpu_custom_call" | custom-call | tf_op jit(solution)/shard_map/layer/pallas_call | solution.py:309
  55.2 1.7 %copy.16 = bf16[64,2048]{1,0:T(8,128)(2,1)} copy(bf16[64,2048]{1,0:T(8,128)(2,1)} %layer.1) | data formatting | bytes 524288

commit v2 on v1

v2 whole, which is shorter than its diff:
```python
import functools

import jax
import jax.numpy as jnp
from jax import lax
from jax.experimental import pallas as pl
from jax.experimental.pallas import tpu as pltpu
from jax.sharding import PartitionSpec as P

MESH = pl.DeviceIdType.MESH
F32, BF16, I32 = jnp.float32, jnp.bfloat16, jnp.int32
SIDE = 4
GROUPS = 4
SLABS = 16
SLOTS = 4
QUARTERS = 4
ROWS = SLABS * QUARTERS * SLOTS
EPS = 1e-06


def distance(offset):
    return sum(min(k, SIDE - k) for k in offset)


def peer_groups():
    every = [(i, j, k) for i in range(SIDE) for j in range(SIDE) for k in range(SIDE)]
    one_way = [o for o in every if distance(o) == 2 and (2 in o or set(o) in ({0, 1}, {0, 3}))]
    first = [o for o in every if distance(o) < 2] + one_way
    second = [o for o in every if distance(o) == 2 and o not in one_way]
    second += [o for o in every if distance(o) == 3 and 2 not in o] + [(2, 1, 0), (2, 3, 0)]
    far = sorted((o for o in every if o not in first and o not in second), key=distance)
    return [first, second, far[0::2], far[1::2]]


PEERS = peer_groups()
PLACE = {o: g * SLABS + i for g, members in enumerate(PEERS) for i, o in enumerate(members)}


def far_first(g):
    return sorted(PEERS[g], key=lambda o: -distance(o))


def iota(shape, dim):
    return lax.broadcasted_iota(I32, shape, dim)


def dot(a, b):
    return jnp.dot(a, b, preferred_element_type=F32)


def kernel(
    res_h, cin_h, gin_h, gout_h, taps_h, oproj_h, gain_h, routes_h, weight_h,
    wg_h, wu_h, wd_h, out_ref,
    taps_ref, gain_ref, routes_ref, weight_ref, cin_v, gin_v, gout_v, res_v, op_v, wg_v, wu_v, wd_v, halo, part, pxr, stream, n4,
    send, taken, rsend, rret, x_v, h_v, mine, theirs, u_v, ut_v, picks, mixes, comb,
    known, in_sem, w_sem, halo_s, halo_r, px_s, px_r, dsp_s, dsp_r, fwd_s, fwd_r, pp_s, pp_r, ret_s, ret_r,
):
    sp, tp = lax.axis_index("sp"), lax.axis_index("tp")
    z, y, x = lax.div(sp, 16), lax.rem(lax.div(sp, 4), 4), lax.rem(sp, 4)
    other = 1 - tp
    rows, tok = cin_v.shape[0], res_v.shape[0]
    width, hidden = out_ref.shape[1], h_v.shape[1]
    piece = width // QUARTERS

    def remote(src, dst, s, r, **where):
        return pltpu.make_async_remote_copy(
            src_ref=src, dst_ref=dst, send_sem=s, recv_sem=r, device_id=where, device_id_type=MESH
        )

    def peer(offset, sign=1):
        dz, dy, dx = (sign * k % SIDE for k in offset)
        return lax.rem(z + dz, SIDE) * 16 + lax.rem(y + dy, SIDE) * 4 + lax.rem(x + dx, SIDE)

    barrier = pltpu.get_barrier_semaphore()
    peers = SIDE**3
    lines = [[tuple(k if a == axis else 0 for a in range(3)) for k in range(1, SIDE)] for axis in range(3)]
    for line in lines:
        for offset in line:
            pl.semaphore_signal(barrier, inc=1, device_id={"sp": peer(offset)}, device_id_type=MESH)
    pl.semaphore_signal(barrier, inc=1, device_id={"tp": other}, device_id_type=MESH)
    pl.semaphore_signal(
        barrier, inc=1, device_id={"sp": lax.rem(sp + peers - 1, peers)}, device_id_type=MESH
    )

    loads = [
        pltpu.make_async_copy(a, b, in_sem.at[i])
        for i, (a, b) in enumerate(
            [
                (routes_h, routes_ref), (cin_h, cin_v), (gin_h, gin_v), (gout_h, gout_v),
                (taps_h, taps_ref), (oproj_h, op_v), (res_h, res_v), (gain_h, gain_ref),
                (weight_h, weight_ref),
            ]
        )
    ]
    for load in loads:
        load.start()
    lanes = QUARTERS * tok
    trow, tcol = iota((tok, lanes), 0), lax.rem(iota((tok, lanes), 1), tok)
    same, before = trow == tcol, trow < tcol
    loads[0].wait()
    diagonal = iota((tok, tok), 0) == iota((tok, tok), 1)

    def upright(line):
        return jnp.sum(jnp.where(diagonal, line, 0.0), axis=1, keepdims=True)

    cols = [upright(routes_ref[k : k + 1].astype(F32)) for k in range(2)]
    keys = []
    for rc in cols:
        rrow = jnp.sum(jnp.where(same, rc, 0.0), axis=0, keepdims=True)
        hits = ((cols[0] == rrow) | (cols[1] == rrow)) & before
        rank = jnp.sum(jnp.where(hits, 1.0, 0.0), axis=0, keepdims=True).astype(I32)
        e = rrow.astype(I32)
        dz = (lax.shift_right_logical(e, 4) + SIDE - z) & 3
        dy = ((lax.shift_right_logical(e, 2) & 3) + SIDE - y) & 3
        dx = ((e & 3) + SIDE - x) & 3
        offset = dz * 16 + dy * 4 + dx
        place = jnp.zeros_like(offset)
        for (i, j, k), where in PLACE.items():
            place = jnp.where(offset == i * 16 + j * 4 + k, where, place)
        keys.append(place * SLOTS + rank)

    with jax.named_scope("meet"):
        pl.semaphore_wait(barrier, 3 * (SIDE - 1) + 2)
    with jax.named_scope("load_a"):
        for load in loads[1:3]:
            load.wait()
    halos = [
        remote(
            v.at[pl.ds(rows - 16, 16)], halo.at[i], halo_s.at[i], halo_r.at[i],
            sp=lax.rem(sp + 1, peers),
        )
        for i, v in enumerate((cin_v, gin_v))
    ]
    for copy in halos:
        copy.start()

    def tell(axis, i):
        for offset in lines[axis]:
            pl.semaphore_signal(
                known.at[i], inc=1, device_id={"sp": peer(offset)}, device_id_type=MESH
            )

    tell(1, 0)

    with jax.named_scope("load_b"):
        for load in loads[3:5]:
            load.wait()
    taps = taps_ref[...].astype(F32)
    t0, t1, t2 = taps[0:1], taps[1:2], taps[2:3]
    mixed = gin_v[...].astype(F32) * cin_v[...].astype(F32)
    row = iota(mixed.shape, 0)
    m1 = jnp.where(row < 1, 0.0, pltpu.roll(mixed, 1, 0))
    m2 = jnp.where(row < 2, 0.0, pltpu.roll(mixed, 2, 0))
    gated = (gout_v[...].astype(F32) * (t0 * m2 + t1 * m1 + t2 * mixed)).astype(BF16)
    with jax.named_scope("load_c"):
        loads[5].wait()
    with jax.named_scope("project"):
        part[...] = dot(gated, op_v[...])
    their_rows = pl.multiple_of(other * tok, tok)
    spans = [(0, 16), (16, tok - 16)]
    swaps = [
        remote(
            part.at[pl.ds(pl.multiple_of(their_rows + lo, 16), n)], pxr.at[pl.ds(lo, n)],
            px_s.at[i], px_r.at[i], tp=other,
        )
        for i, (lo, n) in enumerate(spans)
    ]
    swaps[1].start()

    @pl.when(tp == 0)
    def _():
        swaps[0].start()

    matrices = [(wg_h, wg_v), (wu_h, wu_v), (wd_h, wd_v)]
    for i, (src, dst) in enumerate(matrices):
        size = dst.shape[0] // 4
        for k in range(4):
            cut = pl.ds(k * size, size)
            pltpu.make_async_copy(src.at[0, cut], dst.at[cut], w_sem.at[i]).start()

    with jax.named_scope("known_0"):
        pl.semaphore_wait(known.at[0], SIDE - 1)
    tell(0, 1)

    a, b = iota((ROWS, ROWS), 0), iota((ROWS, ROWS), 1)
    slab_of = lax.shift_right_logical(a, 4) * SLOTS + (a & 3)
    quarter_ok = (lax.shift_right_logical(a, 2) & 3) == lax.shift_right_logical(b, 6)
    for g in range(GROUPS):
        want = slab_of + g * SLABS * SLOTS
        hit = ((keys[0] == want) | (keys[1] == want)) & quarter_ok
        picks[g] = jnp.where(hit, 1.0, 0.0).astype(BF16)

    def plain_to_slab(r):
        q, i, s = lax.shift_right_logical(r, 6), lax.shift_right_logical(r, 2) & 15, r & 3
        return i * 16 + q * 4 + s

    u_v[...] = jnp.where(plain_to_slab(a) == b, 1.0, 0.0).astype(BF16)
    ut_v[...] = jnp.where(plain_to_slab(b) == a, 1.0, 0.0).astype(BF16)
    for load in loads[6:]:
        load.wait()

    def first_rows():
        with jax.named_scope("halo"):
            for copy in halos:
                copy.wait()
        hm = jnp.where(sp > 0, halo[0].astype(F32) * halo[1].astype(F32), 0.0)
        ext = jnp.concatenate([hm, gin_v[0:16].astype(F32) * cin_v[0:16].astype(F32)], axis=0)
        conv = t0 * pltpu.roll(ext, 2, 0)[16:32] + t1 * pltpu.roll(ext, 1, 0)[16:32] + t2 * ext[16:32]
        with jax.named_scope("first"):
            part[0:16] = dot((gout_v[0:16].astype(F32) * conv).astype(BF16), op_v[...])

    def norm():
        with jax.named_scope("swap"):
            for copy in swaps:
                copy.wait_recv()
        s = part[pl.ds(pl.multiple_of(tp * tok, tok), tok)] + pxr[...] + res_v[...].astype(F32)
        stream[...] = s
        inverse = lax.rsqrt(jnp.mean(s * s, axis=-1, keepdims=True) + EPS)
        normed = (s * inverse * gain_ref[...]).astype(BF16)
        for q in range(QUARTERS):
            n4[q * tok : (q + 1) * tok] = normed[:, q * piece : (q + 1) * piece]

    base = tp * GROUPS * SLABS

    def dispatch(g):
        with jax.named_scope(f"pack_{g}"):
            send[g * SLABS : (g + 1) * SLABS] = dot(picks[g], n4[...]).astype(BF16).reshape(SLABS, 16, piece)
        for offset in far_first(g):
            pos = PLACE[offset]
            if distance(offset):
                remote(
                    send.at[pos], taken.at[base + pos], dsp_s, dsp_r.at[g], sp=peer(offset)
                ).start()
            else:
                pltpu.make_async_copy(send.at[pos], taken.at[base + pos], dsp_r.at[g]).start()

    @pl.when(tp == 1)
    def _():
        norm()
        pl.semaphore_wait(known.at[1], SIDE - 1)
        dispatch(0)
        dispatch(1)
        first_rows()
        swaps[0].start()
        dispatch(2)
        dispatch(3)

    @pl.when(tp == 0)
    def _():
        first_rows()
        norm()
        pl.semaphore_wait(known.at[1], SIDE - 1)
        for g in (2, 3, 0, 1):
            dispatch(g)

    def part_of(ref, g, core=0):
        return ref.at[pl.ds(core * GROUPS * SLABS + g * SLABS, SLABS)]

    def arrived(ref, sem, g):
        return remote(part_of(ref, g), part_of(ref, g), sem, sem, tp=other)

    def forward(g):
        return remote(part_of(taken, g, tp), part_of(taken, g, tp), fwd_s.at[g], fwd_r.at[g], tp=other)

    def half(core, g, rows=pl.ds(0, ROWS)):
        return remote(
            mine.at[core * GROUPS + g, rows], theirs.at[g, rows], pp_s.at[g], pp_r.at[g], tp=other
        )

    lane = iota((tok, ROWS), 1)
    lane_slot = lax.shift_right_logical(lane, 4) * SLOTS + (lane & 3)
    lane_quarter = lax.shift_right_logical(lane, 2) & 3
    weights = [upright(weight_ref[k : k + 1]) for k in range(2)]
    key_cols = [upright(k[:, :tok].astype(F32)).astype(I32) for k in keys]
    for g in range(GROUPS):
        want = lane_slot + g * SLABS * SLOTS
        mix = sum(jnp.where(k == want, w, 0.0) for k, w in zip(key_cols, weights))
        high = mix.astype(BF16).astype(F32)
        for i, m in enumerate((high, mix - high)):
            for q in range(QUARTERS):
                at = (i * QUARTERS + q) * tok
                mixes[g, at : at + tok] = jnp.where(lane_quarter == q, m, 0.0).astype(BF16)

    def take(core, g):
        @pl.when(tp == core)
        def _():
            with jax.named_scope(f"take_{core}_{g}"):
                arrived(taken, dsp_r.at[g], g).wait_recv()
            forward(g).start()

    def unpack(core, g, at):
        @pl.when(tp != core)
        def _():
            with jax.named_scope(f"other_{core}_{g}"):
                forward(g).wait_recv()

        start = (core * GROUPS + g) * SLABS
        with jax.named_scope(f"unpack_{core}_{g}"):
            plain = dot(u_v[...], taken[start : start + SLABS].reshape(ROWS, piece)).astype(BF16)
            for q in range(QUARTERS):
                x_v[at : at + tok, q * piece : (q + 1) * piece] = plain[q * tok : (q + 1) * tok]

    def give_back(core, groups):
        @pl.when(tp == core)
        def _():
            for g in groups:
                with jax.named_scope(f"half_{core}_{g}"):
                    half(core, g).wait_recv()
                with jax.named_scope(f"repack_{core}_{g}"):
                    total = (mine[core * GROUPS + g].astype(F32) + theirs[g].astype(F32)).astype(BF16)
                    slabs = dot(ut_v[...], total).astype(BF16)
                    rsend[g * SLABS : (g + 1) * SLABS] = slabs.reshape(SLABS, 16, piece)
                for offset in far_first(g):
                    pos = PLACE[offset]
                    if distance(offset):
                        remote(
                            rsend.at[pos], rret.at[pos], ret_s, ret_r.at[g], sp=peer(offset, -1)
                        ).start()
                    else:
                        pltpu.make_async_copy(rsend.at[pos], rret.at[pos], ret_r.at[g]).start()

    steps = [(1, (0, 1)), (1, (2, 3)), (0, (2, 3)), (0, (0, 1))]
    for g in steps[0][1]:
        take(1, g)
    for step, (core, groups) in enumerate(steps):
        for i, g in enumerate(groups):
            unpack(core, g, i * tok)
        if step == 0:
            with jax.named_scope("weights"):
                for i, (src, dst) in enumerate(matrices[:2]):
                    pltpu.make_async_copy(src.at[0], dst, w_sem.at[i]).wait()
        tiles = hidden // 256
        for n in range(tiles):
            cols = slice(n * 256, (n + 1) * 256)
            gate, up = dot(x_v[...], wg_v[:, cols]), dot(x_v[...], wu_v[:, cols])
            h_v[:, cols] = (gate / (1.0 + jnp.exp(-gate)) * up).astype(BF16)
            if n == tiles // 2 and step:
                give_back(*steps[step - 1])
            if n == (tiles - 1 if step == 1 else tiles // 2) and 0 < step < len(steps) - 1:
                for g in steps[step + 1][1]:
                    take(steps[step + 1][0], g)
        if step == 0:
            pltpu.make_async_copy(wd_h.at[0], wd_v, w_sem.at[2]).wait()
        for q in range(QUARTERS):
            res = dot(h_v[...], wd_v[:, q * piece : (q + 1) * piece]).astype(BF16)
            rows = slice(q * tok, (q + 1) * tok)
            for i, g in enumerate(groups):
                mine[core * GROUPS + g, rows] = res[i * tok : (i + 1) * tok]

            @pl.when(tp != core)
            def _():
                for g in groups:
                    half(core, g, pl.ds(q * tok, tok)).start()

        if step == 0:
            for g in steps[1][1]:
                take(steps[1][0], g)
    give_back(*steps[-1])

    comb[...] = jnp.zeros_like(comb)
    for g in (2, 3, 1, 0):
        with jax.named_scope(f"back_{g}"):
            arrived(rret, ret_r.at[g], g).wait_recv()
        slabs = rret[g * SLABS : (g + 1) * SLABS].reshape(ROWS, piece)
        comb[...] += dot(mixes[g], slabs)
    for q in range(QUARTERS):
        cols = slice(q * piece, (q + 1) * piece)
        routed = comb[q * tok : (q + 1) * tok] + comb[(QUARTERS + q) * tok : (QUARTERS + q + 1) * tok]
        out_ref[:, cols] = (stream[:, cols] + routed).astype(BF16)

    for copy in swaps:
        copy.wait_send()
    rest = pl.ds(1, GROUPS * SLABS - 1)
    remote(send.at[rest], rret.at[rest], dsp_s, dsp_s, tp=other).wait_send()
    remote(rsend.at[rest], rret.at[rest], ret_s, ret_s, tp=other).wait_send()
    for g in range(GROUPS):
        forward(g).wait_send()
        half(0, g).wait_send()


def per_device(
    residual, conv_input, input_gate, output_gate, conv_taps, out_proj, norm_gain, routes,
    route_weight, gate_proj, up_proj, down_proj,
):
    rows, chan = conv_input.shape
    tok, width = residual.shape
    hidden = gate_proj.shape[2]
    piece = width // QUARTERS
    slabs = (GROUPS * SLABS, QUARTERS * SLOTS, piece)
    hbm = pl.BlockSpec(memory_space=pltpu.HBM)
    dma = pltpu.SemaphoreType.DMA
    v = pltpu.VMEM
    return pl.pallas_call(
        kernel,
        out_shape=jax.ShapeDtypeStruct((tok, width), BF16),
        in_specs=[hbm] * 12,
        out_specs=pl.BlockSpec(memory_space=pltpu.VMEM),
        scratch_shapes=[
            v(conv_taps.shape, BF16), v((1, width), F32), v((2, tok), I32), v((2, tok), F32),
            v((rows, chan), BF16), v((rows, chan), BF16), v((rows, chan), BF16),
            v((tok, width), BF16), v((chan, width), BF16),
            v((width, hidden), BF16), v((width, hidden), BF16), v((hidden, width), BF16),
            v((2, 16, chan), BF16), v((rows, width), F32), v((tok, width), F32), v((tok, width), F32),
            v((QUARTERS * tok, piece), BF16),
            v(slabs, BF16), v((2 * slabs[0], *slabs[1:]), BF16), v(slabs, BF16), v(slabs, BF16),
            v((2 * tok, width), BF16), v((2 * tok, hidden), BF16),
            v((2 * GROUPS, ROWS, piece), BF16), v((GROUPS, ROWS, piece), BF16),
            v((ROWS, ROWS), BF16), v((ROWS, ROWS), BF16), v((GROUPS, ROWS, ROWS), BF16),
            v((GROUPS, 2 * ROWS, ROWS), BF16), v((2 * ROWS, piece), F32),
            pltpu.SemaphoreType.REGULAR((2,)), dma((9,)), dma((3,)), dma((2,)), dma((2,)), dma((2,)), dma((2,)),
            dma, dma((GROUPS,)), dma((GROUPS,)), dma((GROUPS,)), dma((GROUPS,)), dma((GROUPS,)),
            dma, dma((GROUPS,)),
        ],
        compiler_params=pltpu.CompilerParams(
            collective_id=0, has_side_effects=True, vmem_limit_bytes=60 * 2**20
        ),
        name="layer",
    )(
        residual, conv_input, input_gate, output_gate, conv_taps, out_proj, norm_gain.reshape(1, -1),
        routes.T, route_weight.T, gate_proj, up_proj, down_proj,
    )


def solution(mesh):
    return jax.shard_map(
        per_device,
        mesh=mesh,
        in_specs=(
            P(("sp", "tp"), None),
            P("sp", "tp"),
            P("sp", "tp"),
            P("sp", "tp"),
            P(None, "tp"),
            P("tp", None),
            P(),
            P(("sp", "tp"), None),
            P(("sp", "tp"), None),
            P("sp", None, "tp"),
            P("sp", None, "tp"),
            P("sp", "tp", None),
        ),
        out_specs=P(("sp", "tp"), None),
        check_vma=False,
    )
```

time: 57.1 us -> 48.1 us (0.84)
  the two profiles are of different devices: /device:TPU:1 before, /device:TPU:0 now
where the time goes in v2:
time: 48.1 us; the launch traced here: 47.9 us
  Pallas kernels  46.2 us (96%)
  local copies, waits for them, and re-layouts  1.67 us (3%)
    pallas_call x1, Pallas kernels, per_device(): pl.pallas_call(kernel, out_shape=jax.ShapeDtypeStruct((tok, width), BF16)...  46.2 us
    unnamed x1, local copies, waits for them, and re-layouts  1.67 us

profile of v2, /device:TPU:0, one launch (start us, length us, event | category | flops | bytes accessed | tf_op | source)
XLA Modules:
  0.0 47.9 jit_solution(17572500304362271917)
XLA Ops:
  0.0 46.2 %layer.1 = bf16[64,2048]{1,0:T(8,128)(2,1)} custom-call(bf16[64,2048]{1,0:T(8,128)(2,1)} %res_h.1, bf16[128,512]{1,0:T(8,128)(2,1)} %cin_h.1, bf16[128,512]{1,0:T(8,128)(2,1)} %gin_h.1, bf16[128,512]{1,0:T(8,128)(2,1)} %gout_h.1, bf16[3,512]{1,0:T(4,128)(2,1)} %taps_h.1, bf16[512,2048]{1,0:T(8,128)(2,1)} %oproj_h.1, f32[1,2048]{1,0:T(1,128)} %bitcast.3, ...), custom_call_target="tpu_custom_call" | custom-call | tf_op jit(solution)/shard_map/layer/pallas_call | solution.py:393
  46.3 1.7 %copy.14 = bf16[64,2048]{1,0:T(8,128)(2,1)} copy(bf16[64,2048]{1,0:T(8,128)(2,1)} %layer.1) | data formatting | bytes 524288

commit v3 on v2

--- a/solution.py
+++ b/solution.py
@@ -250,6 +250,7 @@
         first_rows()
         norm()
         pl.semaphore_wait(known.at[1], SIDE - 1)
+        pl.semaphore_wait(known.at[2], 1)
         for g in (2, 3, 0, 1):
             dispatch(g)
 
@@ -320,8 +321,13 @@
                         pltpu.make_async_copy(rsend.at[pos], rret.at[pos], ret_r.at[g]).start()
 
     steps = [(1, (0, 1)), (1, (2, 3)), (0, (2, 3)), (0, (0, 1))]
-    for g in steps[0][1]:
-        take(1, g)
+    take(1, 0)
+
+    @pl.when(tp == 1)
+    def _():
+        pl.semaphore_signal(known.at[2], inc=1, device_id={"tp": other}, device_id_type=MESH)
+
+    take(1, 1)
     for step, (core, groups) in enumerate(steps):
         for i, g in enumerate(groups):
             unpack(core, g, i * tok)
@@ -347,10 +353,13 @@
             for i, g in enumerate(groups):
                 mine[core * GROUPS + g, rows] = res[i * tok : (i + 1) * tok]
 
-            @pl.when(tp != core)
-            def _():
-                for g in groups:
-                    half(core, g, pl.ds(q * tok, tok)).start()
+            if q == QUARTERS - 1 or (q == QUARTERS // 2 - 1 and step == len(steps) - 1):
+                since = 0 if q < QUARTERS - 1 or step < len(steps) - 1 else QUARTERS // 2
+
+                @pl.when(tp != core)
+                def _():
+                    for g in groups:
+                        half(core, g, pl.ds(since * tok, (q + 1 - since) * tok)).start()
 
         if step == 0:
             for g in steps[1][1]:
@@ -407,7 +416,7 @@
             v((2 * GROUPS, ROWS, piece), BF16), v((GROUPS, ROWS, piece), BF16),
             v((ROWS, ROWS), BF16), v((ROWS, ROWS), BF16), v((GROUPS, ROWS, ROWS), BF16),
             v((GROUPS, 2 * ROWS, ROWS), BF16), v((2 * ROWS, piece), F32),
-            pltpu.SemaphoreType.REGULAR((2,)), dma((9,)), dma((3,)), dma((2,)), dma((2,)), dma((2,)), dma((2,)),
+            pltpu.SemaphoreType.REGULAR((3,)), dma((9,)), dma((3,)), dma((2,)), dma((2,)), dma((2,)), dma((2,)),
             dma, dma((GROUPS,)), dma((GROUPS,)), dma((GROUPS,)), dma((GROUPS,)), dma((GROUPS,)),
             dma, dma((GROUPS,)),
         ],

time: 48.1 us -> 45.6 us (0.948)
  Pallas kernels: 46.2 us -> 43.8 us
    pallas_call x1, Pallas kernels: 46.2 us -> 43.8 us  [per_device(): pl.pallas_call(kernel, out_shape=jax.ShapeDtypeStruct((tok, width), BF16)...]
where the time goes in v3:
time: 45.6 us; the launch traced here: 45.5 us
  Pallas kernels  43.8 us (96%)
  local copies, waits for them, and re-layouts  1.67 us (4%)
    pallas_call x1, Pallas kernels, per_device(): pl.pallas_call(kernel, out_shape=jax.ShapeDtypeStruct((tok, width), BF16)...  43.8 us
    unnamed x1, local copies, waits for them, and re-layouts  1.67 us

profile of v3, /device:TPU:0, one launch (start us, length us, event | category | flops | bytes accessed | tf_op | source)
XLA Modules:
  0.0 45.5 jit_solution(15759138842702699534)
XLA Ops:
  0.0 43.8 %layer.1 = bf16[64,2048]{1,0:T(8,128)(2,1)} custom-call(bf16[64,2048]{1,0:T(8,128)(2,1)} %res_h.1, bf16[128,512]{1,0:T(8,128)(2,1)} %cin_h.1, bf16[128,512]{1,0:T(8,128)(2,1)} %gin_h.1, bf16[128,512]{1,0:T(8,128)(2,1)} %gout_h.1, bf16[3,512]{1,0:T(4,128)(2,1)} %taps_h.1, bf16[512,2048]{1,0:T(8,128)(2,1)} %oproj_h.1, f32[1,2048]{1,0:T(1,128)} %bitcast.3, ...), custom_call_target="tpu_custom_call" | custom-call | tf_op jit(solution)/shard_map/layer/pallas_call | solution.py:402
  43.8 1.7 %copy.14 = bf16[64,2048]{1,0:T(8,128)(2,1)} copy(bf16[64,2048]{1,0:T(8,128)(2,1)} %layer.1) | data formatting | bytes 524288

commit v4 on v3

--- a/solution.py
+++ b/solution.py
@@ -340,7 +340,7 @@
             cols = slice(n * 256, (n + 1) * 256)
             gate, up = dot(x_v[...], wg_v[:, cols]), dot(x_v[...], wu_v[:, cols])
             h_v[:, cols] = (gate / (1.0 + jnp.exp(-gate)) * up).astype(BF16)
-            if n == tiles // 2 and step:
+            if n == (2 if step == 3 else tiles // 2) and step:
                 give_back(*steps[step - 1])
             if n == (tiles - 1 if step == 1 else tiles // 2) and 0 < step < len(steps) - 1:
                 for g in steps[step + 1][1]:
@@ -353,8 +353,8 @@
             for i, g in enumerate(groups):
                 mine[core * GROUPS + g, rows] = res[i * tok : (i + 1) * tok]
 
-            if q == QUARTERS - 1 or (q == QUARTERS // 2 - 1 and step == len(steps) - 1):
-                since = 0 if q < QUARTERS - 1 or step < len(steps) - 1 else QUARTERS // 2
+            if q == QUARTERS - 1 or (q == QUARTERS // 2 - 1 and step >= 2):
+                since = 0 if q < QUARTERS - 1 or step < 2 else QUARTERS // 2
 
                 @pl.when(tp != core)
                 def _():

time: 45.6 us -> 45.7 us (level)
  no operation moved by 1% of the time
where the time goes in v4:
time: 45.7 us; the launch traced here: 45.5 us
  Pallas kernels  43.8 us (96%)
  local copies, waits for them, and re-layouts  1.67 us (4%)
    pallas_call x1, Pallas kernels, per_device(): pl.pallas_call(kernel, out_shape=jax.ShapeDtypeStruct((tok, width), BF16)...  43.8 us
    unnamed x1, local copies, waits for them, and re-layouts  1.67 us

profile of v4, /device:TPU:0, one launch (start us, length us, event | category | flops | bytes accessed | tf_op | source)
XLA Modules:
  0.0 45.5 jit_solution(16617030508902742780)
XLA Ops:
  0.0 43.8 %layer.1 = bf16[64,2048]{1,0:T(8,128)(2,1)} custom-call(bf16[64,2048]{1,0:T(8,128)(2,1)} %res_h.1, bf16[128,512]{1,0:T(8,128)(2,1)} %cin_h.1, bf16[128,512]{1,0:T(8,128)(2,1)} %gin_h.1, bf16[128,512]{1,0:T(8,128)(2,1)} %gout_h.1, bf16[3,512]{1,0:T(4,128)(2,1)} %taps_h.1, bf16[512,2048]{1,0:T(8,128)(2,1)} %oproj_h.1, f32[1,2048]{1,0:T(1,128)} %bitcast.3, ...), custom_call_target="tpu_custom_call" | custom-call | tf_op jit(solution)/shard_map/layer/pallas_call | solution.py:402
  43.9 1.7 %copy.14 = bf16[64,2048]{1,0:T(8,128)(2,1)} copy(bf16[64,2048]{1,0:T(8,128)(2,1)} %layer.1) | data formatting | bytes 524288
